TPU v7x, 32 devices: a whole 2x2x4 slice. The times are simulated.
32 devices in a mesh: tp: 8 (over z, y), dp: 4 (over x, core).
Axes of the slice: x: 2, y: 2, z: 4, core: 2. Of those that a mesh axis runs over, the one named last changes fastest.
Arguments:
- stream: bfloat16 [32, 4096], P('dp', 'tp'), may hold values from -6 to 6
- query_weight: bfloat16 [2, 4096, 3072], P(None, 'dp', 'tp'), may hold values from -0.09375 to 0.09375
- key_weight: bfloat16 [2, 4096, 3072], P(None, 'dp', 'tp'), may hold values from -0.09375 to 0.09375
- value_weight: bfloat16 [2, 4096, 3072], P(None, 'dp', 'tp'), may hold values from -0.09375 to 0.09375
- outgate_weight: bfloat16 [2, 4096, 3072], P(None, 'dp', 'tp'), may hold values from -0.09375 to 0.09375
- gate_weight: bfloat16 [2, 4096, 32], replicated, may hold values from -0.09375 to 0.09375
- gate_bias: float32 [2, 32], replicated, may hold values from -1 to 3
- output_weight: bfloat16 [2, 3072, 4096], P(None, 'dp', 'tp'), may hold values from -0.109375 to 0.109375
- norm_gain: float32 [2, 4096], replicated, may hold values from 0.1 to 1.9
- matrix_state: float32 [2, 32, 192, 16, 192], P(None, 'dp', 'tp'), may hold values from -0.6 to 0.6
- normalizer_state: float32 [2, 32, 16, 192], P(None, 'dp'), may hold values from -0.6 to 0.6
- stabilizer_state: float32 [2, 32, 16], P(None, 'dp'), may hold values from -4 to 4
Outputs:
- out_stream: bfloat16 [32, 4096], P('dp', 'tp')
- new_matrix: float32 [2, 32, 192, 16, 192], P(None, 'dp', 'tp')
- new_normalizer: float32 [2, 32, 16, 192], P(None, 'dp')
- new_stabilizer: float32 [2, 32, 16], P(None, 'dp')
All inputs are finite; a program needn't handle non-finite values.
Results may differ from a plain program's by a relative error of at most 0.015.
Values may be sent and summed in bfloat16 or wider, within the bound.
A program may use at most 128 MiB of HBM per device.

v0:
```python
import jax
import jax.numpy as jnp
from jax import lax
from jax.sharding import PartitionSpec as P

residual_scale = 8.0**0.25
norm_eps = 1e-05


def normalize(values_in, gain):
    upcast = values_in.astype(jnp.float32)
    average = jnp.mean(upcast, axis=-1, keepdims=True)
    variance = jnp.mean(jnp.square(upcast - average), axis=-1, keepdims=True)
    return ((upcast - average) * lax.rsqrt(variance + norm_eps) * gain).astype(jnp.bfloat16)


def widen_rows(local_cols):
    return lax.all_gather(local_cols, "tp", axis=1, tiled=True)


def shards(
    stream,
    query_weight,
    key_weight,
    value_weight,
    outgate_weight,
    gate_weight,
    gate_bias,
    output_weight,
    norm_gain,
    matrix_state,
    normalizer_state,
    stabilizer_state,
):
    head_count = gate_bias.shape[1] // 2
    head_size = normalizer_state.shape[3]
    seq_local = stream.shape[0]
    feat_local = stream.shape[1]
    col_local = query_weight.shape[2]
    feat_offset = lax.axis_index("tp") * feat_local
    x_local = stream
    x_full = widen_rows(stream)
    new_mats, new_norms, new_stabs = ([], [], [])
    for block_no in range(gate_bias.shape[0]):
        weight_set = (
            query_weight[block_no],
            key_weight[block_no],
            value_weight[block_no],
            outgate_weight[block_no],
        )
        columns = x_full
        joined = jnp.concatenate(
            (
                lax.all_gather(weight_set[0], "dp", axis=0, tiled=True),
                lax.all_gather(weight_set[1], "dp", axis=0, tiled=True),
                lax.all_gather(weight_set[2], "dp", axis=0, tiled=True),
                lax.all_gather(weight_set[3], "dp", axis=0, tiled=True),
            ),
            axis=1,
        )
        packed = jnp.dot(columns, joined, preferred_element_type=jnp.float32)
        projected = packed.astype(jnp.bfloat16)
        query_part = projected[:, :col_local]
        key_part = projected[:, col_local : 2 * col_local]
        value_part = projected[:, 2 * col_local : 3 * col_local]
        outgate_part = projected[:, 3 * col_local :]
        query_full, key_full = (
            lax.all_gather(query_part, "tp", axis=1, tiled=True),
            lax.all_gather(key_part, "tp", axis=1, tiled=True),
        )
        gate_pre = (
            jnp.dot(x_full, gate_weight[block_no], preferred_element_type=jnp.float32)
            + gate_bias[block_no]
        )
        log_in = gate_pre[:, :head_count]
        log_forget = jax.nn.log_sigmoid(gate_pre[:, head_count:])
        old_stab = stabilizer_state[block_no]
        stab_new = jnp.maximum(log_forget + old_stab, log_in)
        retain = jnp.exp(log_forget + old_stab - stab_new)
        admit = jnp.exp(log_in - stab_new)
        queries = query_full.astype(jnp.float32).reshape(seq_local, head_count, head_size)
        keys = key_full.astype(jnp.float32).reshape(
            seq_local, head_count, head_size
        ) * head_size ** (-0.5)
        values = value_part.astype(jnp.float32).reshape(seq_local, -1, head_count)
        matrix = (
            retain[:, None, :, None] * matrix_state[block_no]
            + admit[:, None, :, None] * values[..., None] * keys[:, None, :, :]
        )
        norm_new = retain[..., None] * normalizer_state[block_no] + admit[..., None] * keys
        numerator = jnp.einsum("shd,sehd->seh", queries, matrix, precision=lax.Precision.HIGHEST)
        denominator = jnp.sum(queries * norm_new, axis=-1)
        divisor = jnp.maximum(jnp.abs(denominator), 1.0)
        readout = (numerator / divisor[:, None, :]).reshape(seq_local, col_local)
        hidden = (readout * jax.nn.sigmoid(outgate_part.astype(jnp.float32))).astype(jnp.bfloat16)
        hidden_full = lax.all_gather(hidden, "tp", axis=1, tiled=True)
        branch = jnp.dot(
            hidden_full,
            lax.all_gather(output_weight[block_no], "dp", axis=0, tiled=True),
            preferred_element_type=jnp.float32,
        )
        summed = (residual_scale * x_local.astype(jnp.float32) + branch).astype(jnp.bfloat16)
        x_full = normalize(widen_rows(summed), norm_gain[block_no])
        x_local = lax.dynamic_slice_in_dim(x_full, feat_offset, feat_local, 1)
        new_mats.append(matrix)
        new_norms.append(norm_new)
        new_stabs.append(stab_new)
    return (x_local, jnp.stack(new_mats), jnp.stack(new_norms), jnp.stack(new_stabs))


def solution(mesh):
    return jax.shard_map(
        shards,
        mesh=mesh,
        in_specs=(
            P("dp", "tp"),
            P(None, "dp", "tp"),
            P(None, "dp", "tp"),
            P(None, "dp", "tp"),
            P(None, "dp", "tp"),
            P(),
            P(),
            P(None, "dp", "tp"),
            P(),
            P(None, "dp", "tp", None, None),
            P(None, "dp", None, None),
            P(None, "dp", None),
        ),
        out_specs=(
            P("dp", "tp"),
            P(None, "dp", "tp", None, None),
            P(None, "dp", None, None),
            P(None, "dp", None),
        ),
        check_vma=False,
    )
```

profile of v0, /device:TPU:0, one launch (start us, length us, event | category | flops | bytes accessed | tf_op | source)
XLA Modules:
  0.0 442.6 jit_solution(219771178601658571)
XLA Ops:
  7.2 2.8 fusion.75
  10.1 1.3 fusion.76
  11.9 1.3 fusion.77
  13.3 1.3 fusion.78
  15.2 1.3 fusion.74
  19.9 32.4 %all_gather.57 = bf16[8,4096]{1,0:T(8,128)(2,1)S(1)} all-gather(bf16[8,512]{1,0:T(8,128)(2,1)S(1)} %copy-done.11), channel_id=1, replica_groups=mesh['tp'=8,'dp'=4] {'tp'}, dimensions={1}, use_global_device_ids=true | all-gather | bytes 73728 | tf_op jit(solution)/shard_map/all_gather | solution.py:18
  53.9 17.6 %all-gather.23.cloned.1.call-done = bf16[1,4096,384]{2,1,0:T(8,128)(2,1)} async-done(((bf16[1,1024,384]{2,1,0:T(8,128)(2,1)}), bf16[1,4096,384]{2,1,0:T(8,128)(2,1)}) %all-gather.23.cloned.1.call-update) | async-done | bytes 3145744 | tf_op jit(solution)/shard_map/all_gather | solution.py:55
  71.5 30.1 %all-gather.25.cloned.1.call-done = bf16[1,4096,384]{2,1,0:T(8,128)(2,1)} async-done(((bf16[1,1024,384]{2,1,0:T(8,128)(2,1)}), bf16[1,4096,384]{2,1,0:T(8,128)(2,1)}) %all-gather.25.cloned.1.call-update) | async-done | bytes 3145744 | tf_op jit(solution)/shard_map/all_gather | solution.py:56
  101.6 30.0 %all-gather.27.cloned.1.call-done = bf16[1,4096,384]{2,1,0:T(8,128)(2,1)} async-done(((bf16[1,1024,384]{2,1,0:T(8,128)(2,1)}), bf16[1,4096,384]{2,1,0:T(8,128)(2,1)}) %all-gather.27.cloned.1.call-update) | async-done | bytes 3145744 | tf_op jit(solution)/shard_map/all_gather | solution.py:57
  131.6 5.9 %fusion.32 = bf16[8,1536]{1,0:T(8,128)(2,1)S(1)} fusion(bf16[8,4096]{1,0:T(8,128)(2,1)S(1)} %all_gather.57, bf16[4096,384]{1,0:T(8,128)(2,1)} %bitcast.111, bf16[4096,384]{1,0:T(8,128)(2,1)} %bitcast.110, bf16[4096,384]{1,0:T(8,128)(2,1)} %bitcast.109, bf16[4096,384]{1,0:T(8,128)(2,1)} %bitcast.107), kind=kOutput, calls=%fused_computation.33 | convolution fusion | flops 151007232 | bytes 12673024 | tf_op jit(solution)/shard_map/dot_general | solution.py:61
  137.5 30.8 %all_gather.63 = bf16[8,3072]{1,0:T(8,128)(2,1)S(1)} all-gather(bf16[8,384]{1,0:T(8,128)(2,1)S(1)} %get-tuple-element.34), channel_id=1, replica_groups=mesh['tp'=8,'dp'=4] {'tp'}, dimensions={1}, use_global_device_ids=true | all-gather | bytes 55296 | tf_op jit(solution)/shard_map/all_gather | solution.py:68
  168.6 30.8 %all_gather.62 = bf16[8,3072]{1,0:T(8,128)(2,1)S(1)} all-gather(bf16[8,384]{1,0:T(8,128)(2,1)S(1)} %get-tuple-element.35), channel_id=1, replica_groups=mesh['tp'=8,'dp'=4] {'tp'}, dimensions={1}, use_global_device_ids=true | all-gather | bytes 55296 | tf_op jit(solution)/shard_map/all_gather | solution.py:69
  199.5 0.8 reshape.140
  200.6 2.9 fusion.21
  203.5 3.3 fusion.24
  207.0 30.8 %all_gather.64 = bf16[8,3072]{1,0:T(8,128)(2,1)S(1)} all-gather(bf16[8,384]{1,0:T(8,128)(2,1)S(1)} %multiply_convert_fusion.1), channel_id=1, replica_groups=mesh['tp'=8,'dp'=4] {'tp'}, dimensions={1}, use_global_device_ids=true | all-gather | bytes 55296 | tf_op jit(solution)/shard_map/all_gather | solution.py:96
  237.8 2.4 fusion.44
  240.2 30.5 %all_gather.66 = bf16[8,4096]{1,0:T(8,128)(2,1)S(1)} all-gather(bf16[8,512]{1,0:T(8,128)(2,1)S(1)} %fusion.44), channel_id=1, replica_groups=mesh['tp'=8,'dp'=4] {'tp'}, dimensions={1}, use_global_device_ids=true | all-gather | bytes 73728 | tf_op jit(solution)/shard_map/all_gather | solution.py:18
  271.4 11.0 %all-gather.37.cloned.1.call-done = bf16[1,4096,384]{2,1,0:T(8,128)(2,1)} async-done(((bf16[1,1024,384]{2,1,0:T(8,128)(2,1)}), bf16[1,4096,384]{2,1,0:T(8,128)(2,1)}) %all-gather.37.cloned.1.call-update) | async-done | bytes 3145744 | tf_op jit(solution)/shard_map/all_gather | solution.py:57
  282.3 5.9 %fusion.26 = bf16[8,1536]{1,0:T(8,128)(2,1)S(1)} fusion(bf16[8,4096]{1,0:T(8,128)(2,1)S(1)} %fusion.55, bf16[4096,384]{1,0:T(8,128)(2,1)} %bitcast.108, bf16[4096,384]{1,0:T(8,128)(2,1)} %bitcast.106, bf16[4096,384]{1,0:T(8,128)(2,1)} %bitcast.105, bf16[4096,384]{1,0:T(8,128)(2,1)} %bitcast.104), kind=kOutput, calls=%fused_computation.31 | convolution fusion | flops 151007232 | bytes 12673024 | tf_op jit(solution)/shard_map/dot_general | solution.py:61
  288.2 30.8 %all_gather.71 = bf16[8,3072]{1,0:T(8,128)(2,1)S(1)} all-gather(bf16[8,384]{1,0:T(8,128)(2,1)S(1)} %get-tuple-element.32), channel_id=1, replica_groups=mesh['tp'=8,'dp'=4] {'tp'}, dimensions={1}, use_global_device_ids=true | all-gather | bytes 55296 | tf_op jit(solution)/shard_map/all_gather | solution.py:69
  319.1 0.8 reshape.141
  320.0 31.0 %all_gather.72 = bf16[8,3072]{1,0:T(8,128)(2,1)S(1)} all-gather(bf16[8,384]{1,0:T(8,128)(2,1)S(1)} %get-tuple-element.31), channel_id=1, replica_groups=mesh['tp'=8,'dp'=4] {'tp'}, dimensions={1}, use_global_device_ids=true | all-gather | bytes 55296 | tf_op jit(solution)/shard_map/all_gather | solution.py:68
  352.4 2.4 fusion.18
  354.8 3.3 fusion.22
  358.4 32.6 %all_gather.73 = bf16[8,3072]{1,0:T(8,128)(2,1)} all-gather(bf16[8,384]{1,0:T(8,128)(2,1)S(1)} %multiply_convert_fusion), channel_id=1, replica_groups=mesh['tp'=8,'dp'=4] {'tp'}, dimensions={1}, use_global_device_ids=true | all-gather | bytes 55296 | tf_op jit(solution)/shard_map/all_gather | solution.py:96
  390.9 4.5 %multiply_add_fusion.1 = (f32[1,8,24,16,192]{4,3,2,1,0:T(8,128)S(1)}, f32[1,8,24,16,192]{4,3,2,1,0:T(8,128)}) fusion(f32[2,8,24,16,192]{4,3,2,1,0:T(8,128)} %param.21, f32[8,16,192]{2,1,0:T(8,128)S(1)} %get-tuple-element.25, f32[8,24,16]{2,1,0:T(8,128)S(1)} %broadcast_multiply_fusion.3, f32[8,16]{1,0:T(8,128)S(1)} %get-tuple-element.39, ...), kind=kLoop, calls=%fused_computation.30 | loop fusion | flops 3538944 | bytes 9659392 | tf_op jit(solution)/shard_map/add | solution.py:87
  395.5 2.6 fusion.41
  398.0 30.5 %all_gather.75 = bf16[8,4096]{1,0:T(8,128)(2,1)S(1)} all-gather(bf16[8,512]{1,0:T(8,128)(2,1)S(1)} %fusion.41), channel_id=1, replica_groups=mesh['tp'=8,'dp'=4] {'tp'}, dimensions={1}, use_global_device_ids=true | all-gather | bytes 73728 | tf_op jit(solution)/shard_map/all_gather | solution.py:18
  428.9 1.0 multiply_add_fusion.3
  430.0 0.7 pad_maximum_fusion.1
  430.7 3.7 pad_maximum_fusion
  (104 shorter events, 11.0 us)
Async XLA Ops:
  7.2 2.9 copy-start.1
  7.2 46.7 %all-gather.21.cloned.1.call-start = ((), (), s32[]{:S(2)}) async-start(), calls=%async_computation | async-start | bytes 3932160 | tf_op jit(solution)/shard_map/all_gather | solution.py:54
  10.0 1.9 copy-start.2
  10.0 61.5 %all-gather.23.cloned.1.call-start = ((), (), s32[]{:S(2)}) async-start(), calls=%async_computation.1 | async-start | bytes 3932160 | tf_op jit(solution)/shard_map/all_gather | solution.py:55
  11.4 1.9 copy-start.3
  11.4 90.2 %all-gather.25.cloned.1.call-start = ((), (), s32[]{:S(2)}) async-start(), calls=%async_computation.2 | async-start | bytes 3932160 | tf_op jit(solution)/shard_map/all_gather | solution.py:56
  13.2 1.9 copy-start.4
  13.3 118.3 %all-gather.27.cloned.1.call-start = ((), (), s32[]{:S(2)}) async-start(), calls=%async_computation.3 | async-start | bytes 3932160 | tf_op jit(solution)/shard_map/all_gather | solution.py:57
  14.7 223.1 %all-gather.29.cloned.1.call-start = ((), (), s32[]{:S(2)}) async-start(), calls=%async_computation.4 | async-start | bytes 3932160 | tf_op jit(solution)/shard_map/all_gather | solution.py:99
  16.4 3.5 copy-start.11
  16.4 35.8 %copy-start.17 = (f32[2,32]{1,0:T(2,128)S(1)}, f32[2,32]{1,0:T(2,128)}, u32[]{:S(2)}) copy-start(f32[2,32]{1,0:T(2,128)} %param.18) | copy-start | bytes 772
  16.4 35.8 %copy-start.12 = (f32[2,4096]{1,0:T(2,128)S(1)}, f32[2,4096]{1,0:T(2,128)}, u32[]{:S(2)}) copy-start(f32[2,4096]{1,0:T(2,128)} %param.20) | copy-start | bytes 98308
  16.5 35.9 %copy-start.9 = (bf16[2,4096,32]{1,2,0:T(8,128)(2,1)S(1)}, bf16[2,4096,32]{1,2,0:T(8,128)(2,1)}, u32[]{:S(2)}) copy-start(bf16[2,4096,32]{1,2,0:T(8,128)(2,1)} %param.17) | copy-start | bytes 1572868
  16.5 36.0 %copy-start.15 = (f32[2,8,16]{2,1,0:T(8,128)S(1)}, f32[2,8,16]{2,1,0:T(8,128)}, u32[]{:S(2)}) copy-start(f32[2,8,16]{2,1,0:T(8,128)} %param.23) | copy-start | bytes 3076
  16.5 254.8 %all-gather.31.cloned.1.call-start = ((), (), s32[]{:S(2)}) async-start(), calls=%async_computation.5 | async-start | bytes 3932160 | tf_op jit(solution)/shard_map/all_gather | solution.py:54
  17.1 254.3 %all-gather.33.cloned.1.call-start = ((), (), s32[]{:S(2)}) async-start(), calls=%async_computation.6 | async-start | bytes 3932160 | tf_op jit(solution)/shard_map/all_gather | solution.py:55
  17.8 253.5 %all-gather.35.cloned.1.call-start = ((), (), s32[]{:S(2)}) async-start(), calls=%async_computation.7 | async-start | bytes 3932160 | tf_op jit(solution)/shard_map/all_gather | solution.py:56
  18.6 263.8 %all-gather.37.cloned.1.call-start = ((), (), s32[]{:S(2)}) async-start(), calls=%async_computation.8 | async-start | bytes 3932160 | tf_op jit(solution)/shard_map/all_gather | solution.py:57
  19.3 376.1 %all-gather.39.cloned.1.call-start = ((), (), s32[]{:S(2)}) async-start(), calls=%async_computation.9 | async-start | bytes 3932160 | tf_op jit(solution)/shard_map/all_gather | solution.py:99
  131.6 68.9 %copy-start.5 = (f32[2,8,16,192]{3,2,1,0:T(8,128)S(1)}, f32[2,8,16,192]{3,2,1,0:T(8,128)}, u32[]{:S(2)}) copy-start(f32[2,8,16,192]{3,2,1,0:T(8,128)} %param.22) | copy-start | bytes 589828
  271.3 80.1 %copy-start.10 = (bf16[8,4096]{1,0:T(8,128)(2,1)}, bf16[8,4096]{1,0:T(8,128)(2,1)S(1)}, u32[]{:S(2)}) copy-start(bf16[8,4096]{1,0:T(8,128)(2,1)S(1)} %fusion.55) | copy-start | bytes 196612
  352.2 6.1 %copy-start.7 = (f32[8,24,16]{2,1,0:T(8,128)}, f32[8,24,16]{2,1,0:T(8,128)S(1)}, u32[]{:S(2)}) copy-start(f32[8,24,16]{2,1,0:T(8,128)S(1)} %broadcast_multiply_fusion.2) | copy-start | bytes 36868
  395.4 33.5 %copy-start.6 = (f32[2,8,16,192]{3,2,1,0:T(8,128)S(1)}, f32[2,8,16,192]{3,2,1,0:T(8,128)}, u32[]{:S(2)}) copy-start(f32[2,8,16,192]{3,2,1,0:T(8,128)} %param.22) | copy-start | bytes 589828
  395.4 33.5 %copy-start.8 = (f32[1,8,16,192]{3,2,1,0:T(8,128)S(1)}, f32[1,8,16,192]{3,2,1,0:T(8,128)}, u32[]{:S(2)}) copy-start(f32[1,8,16,192]{3,2,1,0:T(8,128)} %reshape.140) | copy-start | bytes 294916
  395.4 35.3 %copy-start = (f32[1,8,24,16,192]{4,3,2,1,0:T(8,128)S(1)}, f32[1,8,24,16,192]{4,3,2,1,0:T(8,128)}, u32[]{:S(2)}) copy-start(f32[1,8,24,16,192]{4,3,2,1,0:T(8,128)} %get-tuple-element.9) | copy-start | bytes 7077892
  430.7 3.7 copy-start.13
  430.7 3.7 copy-start.14
  430.7 4.4 copy-start.16
Sparse Core Ops, SparseCore 0:
  10.1 31.2 all-gather.20
  43.0 28.4 all-gather.22
  73.1 28.4 all-gather.24
  103.0 28.4 all-gather.26
  133.0 28.4 all-gather.28
  162.9 28.4 all-gather.30
  193.0 28.4 all-gather.32
  223.1 28.4 all-gather.34
  253.8 28.4 all-gather.36
  283.8 28.4 all-gather.38
where the time goes:
time: 443 us
  blocking collectives  280 us (63%)
  waiting for transfers between devices  92 us (21%)
  matrix products  23.7 us (5%)
  other arithmetic  19.2 us (4%)
  between operations  14.6 us (3%)
  local copies, waits for them, and re-layouts  12.6 us (3%)
    all_gather x3, blocking collectives, widen_rows(): return lax.all_gather(local_cols, 'tp', axis=1, tiled=True)  93.4 us
    all_gather x2, blocking collectives, shards(): hidden_full = lax.all_gather(hidden, 'tp', axis=1, tiled=True)  63.3 us
    all_gather x2, blocking collectives, shards(): lax.all_gather(query_part, 'tp', axis=1, tiled=True)  61.8 us
    all_gather x2, blocking collectives, shards(): lax.all_gather(key_part, 'tp', axis=1, tiled=True)  61.6 us
    all_gather x2, waiting for transfers between devices, shards(): lax.all_gather(weight_set[3], 'dp', axis=0, tiled=True)  40.9 us
    all_gather x2, waiting for transfers between devices, shards(): lax.all_gather(weight_set[2], 'dp', axis=0, tiled=True)  30.1 us
    all_gather x2, waiting for transfers between devices, shards(): lax.all_gather(weight_set[1], 'dp', axis=0, tiled=True)  17.7 us
    dot_general x2, matrix products, shards(): packed = jnp.dot(columns, joined, preferred_element_type=jnp.float32)  11.8 us
  transfers between devices with their start and end apart: 10, of which 4 were waited for; matrix products, arithmetic and copies ran while one was open for 10% of the time, Pallas kernels for 0%

commit v1 on v0

v1 whole, which is shorter than its diff:
```python
import functools
import math

import jax
import jax.numpy as jnp
from jax import lax
from jax.experimental import pallas as pl
from jax.experimental.pallas import tpu as pltpu
from jax.sharding import PartitionSpec as P

residual_scale = 8.0**0.25
norm_eps = 1e-05
f32, bf16 = jnp.float32, jnp.bfloat16
STREAM, QK, GATE, VO, HEAD, HID, OUT, STAT = range(8)


def each(count, step):
    if count <= 8:
        for k in range(count):
            step(k)
    else:

        def body(k, carry):
            step(k)
            return carry

        lax.fori_loop(0, count, body, 0)


def kernel(
    tp,
    dp,
    stream,
    wq,
    wk,
    wv,
    wo,
    gate_weight,
    gate_bias,
    out_weight,
    norm_gain,
    matrix_in,
    normal_in,
    stab_in,
    stream_out,
    matrix_out,
    normal_out,
    stab_out,
    x_own,
    w_in,
    w_gate,
    bias,
    w_out,
    gain,
    matrix,
    normal,
    stab,
    x_all,
    qk_part,
    qk_recv,
    g_part,
    g_recv,
    vo_part,
    vo_recv,
    head_own,
    head_all,
    hid_own,
    hid_all,
    out_part,
    out_recv,
    stat_own,
    stat_all,
    y_own,
    queries_ref,
    keys_ref,
    result,
    load_sem,
    store_sem,
    send_sem,
    recv_sem,
):
    blocks, seqs, chans, heads, size = matrix.shape
    feats = x_own.shape[1]
    cols = w_in.shape[3]
    ratio = tp // dp
    width = head_all.shape[-1]
    pieces = cols // width
    per_head = size // width
    ti, di = lax.axis_index("tp"), lax.axis_index("dp")
    group = ti // ratio
    place = ti - group * ratio
    home = group == di
    model = tp * feats

    loads = []

    def load(src, dst):
        copy = pltpu.make_async_copy(src, dst, load_sem.at[len(loads)])
        copy.start()
        loads.append(copy)
        return copy

    rows = w_gate.shape[1]
    got_x = load(stream, x_own)
    got_w, got_gate, got_out, got_matrix = [], [], [], []
    for b in range(blocks):
        got_w.append([load(w.at[b], w_in.at[b, n]) for n, w in enumerate((wq, wk, wv, wo))])
        got_gate.append(load(gate_weight.at[b, pl.ds(pl.multiple_of(di * rows, rows), rows)], w_gate.at[b]))
        if b == 0:
            got_small = [load(gate_bias, bias), load(norm_gain, gain), load(normal_in, normal), load(stab_in, stab)]
        got_matrix.append(load(matrix_in.at[b], matrix.at[b]))
        got_out.append(load(out_weight.at[b], w_out.at[b]))

    barrier = pltpu.get_barrier_semaphore()

    def greet(k):
        other = lax.rem(ti * dp + di + 1 + k, tp * dp)
        pl.semaphore_signal(
            barrier,
            inc=1,
            device_id={"tp": other // dp, "dp": lax.rem(other, dp)},
            device_id_type=pl.DeviceIdType.MESH,
        )

    each(tp * dp - 1, greet)
    pl.semaphore_wait(barrier, tp * dp - 1)

    unsent = []

    def send(src, dst, b, phase, where):
        pltpu.make_async_remote_copy(
            src_ref=src,
            dst_ref=dst,
            send_sem=send_sem.at[b, phase],
            recv_sem=recv_sem.at[b, phase],
            device_id=where,
            device_id_type=pl.DeviceIdType.MESH,
        ).start()

    def await_bytes(ref, sem):
        pltpu.make_async_copy(ref, ref, sem).wait()

    def to_tp(src, dst, b, phase):
        each(tp - 1, lambda k: send(src, dst, b, phase, {"tp": lax.rem(ti + 1 + k, tp), "dp": di}))
        unsent.append((tp - 1, src, b, phase, None))

    def to_dp(part, recv, b, phase):
        def one(k):
            other = lax.rem(di + 1 + k, dp)
            send(part.at[b, other], recv.at[b, di], b, phase, {"tp": ti, "dp": other})

        each(dp - 1, one)
        unsent.append((dp - 1, part.at[b, 0], b, phase, None))

    def to_group(src, slots, b, phase):
        dst = slots.at[b, place * dp + di]

        def one(k):
            send(src, dst, b, phase, {"tp": lax.rem(ti + 1 + k, tp), "dp": group})

        each(tp - 1, one)

        @pl.when(jnp.logical_not(home))
        def _():
            send(src, dst, b, phase, {"tp": ti, "dp": group})

        @pl.when(home)
        def _():
            slots[b, place * dp + di] = src[...]

        unsent.append((tp - 1, src, b, phase, jnp.logical_not(home)))

    def from_group(slots, b, phase):
        @pl.when(home)
        def _():
            await_bytes(slots.at[b, pl.ds(0, tp - 1)], recv_sem.at[b, phase])

        @pl.when(jnp.logical_not(home))
        def _():
            await_bytes(slots.at[b], recv_sem.at[b, phase])

    def rows_of(slots, b, c):
        held = slots[b, c * dp : (c + 1) * dp].astype(f32)
        return held.reshape(dp * seqs, held.shape[-1])

    def moments(stats):
        means, squares = stats[..., 0:1], stats[..., 1:2]
        mean = jnp.sum(means, axis=-3) * (1.0 / tp)
        apart = means - jnp.expand_dims(mean, -3)
        variance = (jnp.sum(squares, axis=-3) + feats * jnp.sum(apart * apart, axis=-3)) * (1.0 / model)
        return mean, lax.rsqrt(variance + norm_eps)

    def gain_of(b, chunk):
        if len(gain.shape) == 2:
            return gain[b : b + 1, pl.ds(pl.multiple_of(chunk * feats, feats), feats)]
        return gain[b, pl.ds(chunk, 1), :]

    got_x.wait()
    to_group(x_own, x_all, 0, STREAM)
    own = x_own[...].astype(f32)
    outs = []

    def store(src, dst):
        copy = pltpu.make_async_copy(src, dst, store_sem.at[len(outs)])
        copy.start()
        outs.append(copy)

    for b in range(blocks):
        if b == 0:
            for copy in got_w[b][:2]:
                copy.wait()
        from_group(x_all, b, STREAM)
        chunks = [rows_of(x_all, b, c) for c in range(ratio)]
        if b > 0:
            await_bytes(stat_all.at[b - 1, pl.ds(0, tp * dp - 1)], recv_sem.at[b - 1, STAT])
            mean, scale = moments(stat_all[b - 1].reshape(dp, tp, seqs, 128))
            mean, scale = mean.reshape(dp * seqs, 1), scale.reshape(dp * seqs, 1)
            chunks = [
                (chunk - mean) * scale * gain_of(b - 1, di * ratio + c) for c, chunk in enumerate(chunks)
            ]
        chunks = [chunk.astype(bf16) for chunk in chunks]

        def project(w, depth=feats):
            return sum(
                jnp.dot(chunk, w[c * depth : (c + 1) * depth, :], preferred_element_type=f32)
                for c, chunk in enumerate(chunks)
            )

        if b > 0:
            for copy in got_w[b][:2]:
                copy.wait()
        for n in range(2):
            qk_part[b, :, n] = project(w_in.at[b, n]).reshape(dp, seqs, cols)
        qk_recv[b, di] = qk_part[b, di]
        to_dp(qk_part, qk_recv, b, QK)
        got_gate[b].wait()
        g_part[b] = project(w_gate.at[b]).reshape(dp, seqs, 2 * heads)
        g_recv[b, di] = g_part[b, di]
        to_dp(g_part, g_recv, b, GATE)
        for copy in got_w[b][2:]:
            copy.wait()
        for n in range(2):
            vo_part[b, :, n] = project(w_in.at[b, 2 + n]).reshape(dp, seqs, cols)
        vo_recv[b, di] = vo_part[b, di]
        to_dp(vo_part, vo_recv, b, VO)
        if b > 0:
            m_own, s_own = moments(stat_all[b - 1, pl.ds(di * tp, tp)])
            own = ((y_own[b - 1].astype(f32) - m_own) * s_own * gain_of(b - 1, ti)).astype(bf16).astype(f32)

        await_bytes(qk_recv.at[b, pl.ds(0, dp - 1)], recv_sem.at[b, QK])
        for n in range(2):
            total = jnp.sum(qk_recv[b, :, n], axis=0)
            for p in range(pieces):
                head_own[b, n, p] = total[:, p * width : (p + 1) * width].astype(bf16)
        head_all[b, ti] = head_own[b]
        to_tp(head_own.at[b], head_all.at[b, ti], b, HEAD)

        await_bytes(g_recv.at[b, pl.ds(0, dp - 1)], recv_sem.at[b, GATE])
        if b == 0:
            for copy in got_small:
                copy.wait()
        pre = jnp.sum(g_recv[b], axis=0) + bias[b : b + 1, :]
        log_in = pre[:, :heads]
        raw = pre[:, heads:]
        log_forget = jnp.minimum(raw, 0.0) - jnp.log1p(jnp.exp(-jnp.abs(raw)))
        carried = log_forget + stab[b]
        stab_new = jnp.maximum(carried, log_in)
        stab[b] = stab_new
        retain = jnp.exp(carried - stab_new).T
        admit = jnp.exp(log_in - stab_new).T
        await_bytes(vo_recv.at[b, pl.ds(0, dp - 1)], recv_sem.at[b, VO])
        value = jnp.sum(vo_recv[b, :, 0], axis=0).astype(bf16).astype(f32).T
        outgate = jnp.sum(vo_recv[b, :, 1], axis=0).astype(bf16).astype(f32)
        opened = jax.nn.sigmoid(outgate)
        got_matrix[b].wait()

        await_bytes(head_all.at[b, pl.ds(0, tp - 1)], recv_sem.at[b, HEAD])
        for h in range(heads):
            for n, ref in ((0, queries_ref), (1, keys_ref)):
                parts = [
                    head_all[b, g // pieces, n, g % pieces].astype(f32)
                    for g in range(h * per_head, (h + 1) * per_head)
                ]
                whole = parts[0] if per_head == 1 else jnp.concatenate(parts, axis=-1)
                if n == 1:
                    whole = whole * size ** (-0.5)
                ref[:, h, :] = whole

        lane = lax.broadcasted_iota(jnp.int32, (chans * heads, seqs), 1)
        readout = jnp.zeros((chans * heads, seqs), f32)
        for s in range(seqs):
            q, k = queries_ref[s], keys_ref[s]
            keep, take = retain[:, s : s + 1], admit[:, s : s + 1]
            norm_new = keep * normal[b, s] + take * k
            normal[b, s] = norm_new
            divisor = jnp.maximum(jnp.abs(jnp.sum(q * norm_new, axis=-1, keepdims=True)), 1.0)
            v = value[:, s : s + 1].reshape(chans, heads, 1)
            new = keep[None] * matrix[b, s] + (take[None] * v) * k[None]
            matrix[b, s] = new
            read = jnp.sum(q[None] * new, axis=-1, keepdims=True) / divisor[None]
            readout = jnp.where(lane == s, read.reshape(chans * heads, 1), readout)
        hid_own[b] = (readout.T * opened).astype(bf16)
        to_group(hid_own.at[b], hid_all, b, HID)
        store(matrix.at[b], matrix_out.at[b])

        got_out[b].wait()
        from_group(hid_all, b, HID)
        chunks = [rows_of(hid_all, b, c).astype(bf16) for c in range(ratio)]
        out_part[b] = project(w_out.at[b], cols).reshape(dp, seqs, feats)
        out_recv[b, di] = out_part[b, di]
        to_dp(out_part, out_recv, b, OUT)
        await_bytes(out_recv.at[b, pl.ds(0, dp - 1)], recv_sem.at[b, OUT])
        y = (residual_scale * own + jnp.sum(out_recv[b], axis=0)).astype(bf16)
        y_own[b] = y
        if b + 1 < blocks:
            to_group(y_own.at[b], x_all, b + 1, STREAM)
        y = y.astype(f32)
        mean = jnp.mean(y, axis=-1, keepdims=True)
        square = jnp.sum(jnp.square(y - mean), axis=-1, keepdims=True)
        at = lax.broadcasted_iota(jnp.int32, (seqs, 128), 1)
        stat = jnp.where(at == 0, mean, square)
        stat_own[b] = stat
        stat_all[b, di * tp + ti] = stat

        if b + 1 < blocks:

            def tell(k, b=b):
                other = lax.rem(ti * dp + di + 1 + k, tp * dp)
                send(
                    stat_own.at[b],
                    stat_all.at[b, di * tp + ti],
                    b,
                    STAT,
                    {"tp": other // dp, "dp": lax.rem(other, dp)},
                )

            each(tp * dp - 1, tell)
            unsent.append((tp * dp - 1, stat_own.at[b], b, STAT, None))
        else:
            to_tp(stat_own.at[b], stat_all.at[b, di * tp + ti], b, STAT)
            store(normal, normal_out)
            store(stab, stab_out)
            await_bytes(stat_all.at[b, pl.ds(0, tp - 1)], recv_sem.at[b, STAT])
            mean, scale = moments(stat_all[b, pl.ds(di * tp, tp)])
            result[...] = ((y - mean) * scale * gain_of(b, ti)).astype(bf16)
            store(result, stream_out)

    for count, src, b, phase, also in unsent:
        each(count, lambda k: await_bytes(src, send_sem.at[b, phase]))
        if also is not None:

            @pl.when(also)
            def _():
                await_bytes(src, send_sem.at[b, phase])

    for copy in outs:
        copy.wait()


def shards(
    tp,
    dp,
    stream,
    query_weight,
    key_weight,
    value_weight,
    outgate_weight,
    gate_weight,
    gate_bias,
    output_weight,
    norm_gain,
    matrix_state,
    normalizer_state,
    stabilizer_state,
):
    blocks, seqs, chans, heads, size = matrix_state.shape
    feats = stream.shape[1]
    _, rows, cols = query_weight.shape
    ratio = tp // dp
    width = math.gcd(cols, size)
    pieces = cols // width
    if feats % 128:
        norm_gain = norm_gain.reshape(blocks, tp, feats)
    vmem = pltpu.VMEM
    anywhere = pl.BlockSpec(memory_space=pl.ANY)
    scratch = [
        vmem((seqs, feats), bf16),
        vmem((blocks, 4, rows, cols), bf16),
        vmem((blocks, rows, 2 * heads), bf16),
        vmem(gate_bias.shape, f32),
        vmem(output_weight.shape, bf16),
        vmem(norm_gain.shape, f32),
        vmem(matrix_state.shape, f32),
        vmem(normalizer_state.shape, f32),
        vmem(stabilizer_state.shape, f32),
        vmem((blocks, ratio * dp, seqs, feats), bf16),
        vmem((blocks, dp, 2, seqs, cols), f32),
        vmem((blocks, dp, 2, seqs, cols), f32),
        vmem((blocks, dp, seqs, 2 * heads), f32),
        vmem((blocks, dp, seqs, 2 * heads), f32),
        vmem((blocks, dp, 2, seqs, cols), f32),
        vmem((blocks, dp, 2, seqs, cols), f32),
        vmem((blocks, 2, pieces, seqs, width), bf16),
        vmem((blocks, tp, 2, pieces, seqs, width), bf16),
        vmem((blocks, seqs, cols), bf16),
        vmem((blocks, ratio * dp, seqs, cols), bf16),
        vmem((blocks, dp, seqs, feats), f32),
        vmem((blocks, dp, seqs, feats), f32),
        vmem((blocks, seqs, 128), f32),
        vmem((blocks, dp * tp, seqs, 128), f32),
        vmem((blocks, seqs, feats), bf16),
        vmem((seqs, heads, size), f32),
        vmem((seqs, heads, size), f32),
        vmem((seqs, feats), bf16),
        pltpu.SemaphoreType.DMA((5 + 7 * blocks,)),
        pltpu.SemaphoreType.DMA((3 + blocks,)),
        pltpu.SemaphoreType.DMA((blocks, 8)),
        pltpu.SemaphoreType.DMA((blocks, 8)),
    ]
    return pl.pallas_call(
        functools.partial(kernel, tp, dp),
        out_shape=(
            jax.ShapeDtypeStruct(stream.shape, stream.dtype),
            jax.ShapeDtypeStruct(matrix_state.shape, f32),
            jax.ShapeDtypeStruct(normalizer_state.shape, f32),
            jax.ShapeDtypeStruct(stabilizer_state.shape, f32),
        ),
        in_specs=[anywhere] * 12,
        out_specs=(anywhere,) * 4,
        scratch_shapes=scratch,
        compiler_params=pltpu.CompilerParams(
            collective_id=0, has_side_effects=True, vmem_limit_bytes=60 * 1024 * 1024
        ),
    )(
        stream,
        query_weight,
        key_weight,
        value_weight,
        outgate_weight,
        gate_weight,
        gate_bias,
        output_weight,
        norm_gain,
        matrix_state,
        normalizer_state,
        stabilizer_state,
    )


def solution(mesh):
    return jax.shard_map(
        functools.partial(shards, mesh.shape["tp"], mesh.shape["dp"]),
        mesh=mesh,
        in_specs=(
            P("dp", "tp"),
            P(None, "dp", "tp"),
            P(None, "dp", "tp"),
            P(None, "dp", "tp"),
            P(None, "dp", "tp"),
            P(),
            P(),
            P(None, "dp", "tp"),
            P(),
            P(None, "dp", "tp", None, None),
            P(None, "dp", None, None),
            P(None, "dp", None),
        ),
        out_specs=(
            P("dp", "tp"),
            P(None, "dp", "tp", None, None),
            P(None, "dp", None, None),
            P(None, "dp", None),
        ),
        check_vma=False,
    )
```

time: 443 us -> 70.7 us (0.16)
  blocking collectives: 280 us -> 0 us
  waiting for transfers between devices: 92 us -> 0 us
  Pallas kernels: 0 us -> 58.1 us
  matrix products: 23.7 us -> 0 us
  other arithmetic: 19.2 us -> 0 us
  between operations: 14.6 us -> 0.64 us
    all_gather x9 -> x0, blocking collectives: 280 us -> none  [the longest x3 93.4 us: widen_rows(): return lax.all_gather(local_cols, 'tp', axis=1, tiled=True)]
    all_gather x10 -> x0, waiting for transfers between devices: 88.8 us -> none  [the longest x2 40.9 us: shards(): lax.all_gather(weight_set[3], 'dp', axis=0, tiled=True)]
    pallas_call x0 -> x1, Pallas kernels: none -> 58.1 us  [shards(): pl.pallas_call(functools.partial(kernel, tp, dp), out_shape=(jax.ShapeDty...]
    dot_general x8 -> x0, matrix products: 23.7 us -> none  [the longest x2 11.8 us: shards(): packed = jnp.dot(columns, joined, preferred_element_type=jnp.float32)]
    unnamed x36 -> x9, local copies, waits for them, and re-layouts: 0.93 us -> 11.7 us
    add x4 -> x0, other arithmetic: 10.8 us -> none  [the longest x3 9.72 us: shards(): retain[:, None, :, None] * matrix_state[block_no]]
    slice x6 -> x0, local copies, waits for them, and re-layouts: 8.06 us -> none  [the longest x1 2.77 us: shards(): query_weight[block_no]]
    another operation x5 -> x0, other arithmetic: 5.07 us -> none  [the longest x1 3.74 us: shards(): jnp.stack(new_mats)]
  transfers between devices with their start and end apart: 10 -> 0, of which waited for: 4 -> 0; matrix products, arithmetic and copies ran while one was open for 10% -> 0% of each run, Pallas kernels for 0% -> 0%
where the time goes in v1:
time: 70.7 us; the launch traced here: 70.5 us
  Pallas kernels  58.1 us (82%)
  local copies, waits for them, and re-layouts  11.7 us (17%)
    pallas_call x1, Pallas kernels, shards(): pl.pallas_call(functools.partial(kernel, tp, dp), out_shape=(jax.ShapeDty...  58.1 us
    unnamed x9, local copies, waits for them, and re-layouts  11.7 us

profile of v1, /device:TPU:0, one launch (start us, length us, event | category | flops | bytes accessed | tf_op | source)
XLA Modules:
  0.0 70.5 jit_solution(4893915969051005123)
XLA Ops:
  0.6 2.6 %copy.16.gate_weight = bf16[2,4096,32]{2,1,0:T(8,128)(2,1)} copy(bf16[2,4096,32]{1,2,0:T(8,128)(2,1)} %param.17) | data formatting | bytes 1048576 | tf_op args[5]
  3.3 58.1 %shard_map.147 = (bf16[8,512]{1,0:T(8,128)(2,1)}, f32[2,8,24,16,192]{4,3,2,1,0:T(8,128)}, f32[2,8,16,192]{3,2,1,0:T(8,128)}, f32[2,8,16]{2,1,0:T(8,128)}) custom-call(bf16[8,512]{1,0:T(8,128)(2,1)} %stream.1, bf16[2,1024,384]{2,1,0:T(8,128)(2,1)} %wq.1, bf16[2,1024,384]{2,1,0:T(8,128)(2,1)} %wk.1, bf16[2,1024,384]{2,1,0:T(8,128)(2,1)} %wv.1, ...), custom_call_target="tpu_custom_call" | custom-call | tf_op jit(solution)/shard_map/pallas_call | solution.py:420
  61.4 1.3 %copy.21 = bf16[8,512]{1,0:T(8,128)(2,1)} copy(bf16[8,512]{1,0:T(8,128)(2,1)} %get-tuple-element.8) | data formatting | bytes 16384
  62.7 0.0 copy-start
  62.7 0.0 copy-start.1
  62.7 6.5 %copy.22 = f32[2,8,24,16,192]{4,3,2,1,0:T(8,128)} copy(f32[2,8,24,16,192]{4,3,2,1,0:T(8,128)} %get-tuple-element.9) | data formatting | bytes 9437184
  69.2 0.0 copy-done
  69.2 0.7 copy.23
  69.9 0.0 copy-done.1
  69.9 0.6 copy.24
Async XLA Ops:
  62.7 6.5 %copy-start = (f32[2,8,16,192]{3,2,1,0:T(8,128)S(1)}, f32[2,8,16,192]{3,2,1,0:T(8,128)}, u32[]{:S(2)}) copy-start(f32[2,8,16,192]{3,2,1,0:T(8,128)} %get-tuple-element.10) | copy-start | bytes 589828
  62.7 7.2 %copy-start.1 = (f32[2,8,16]{2,1,0:T(8,128)S(1)}, f32[2,8,16]{2,1,0:T(8,128)}, u32[]{:S(2)}) copy-start(f32[2,8,16]{2,1,0:T(8,128)} %get-tuple-element.11) | copy-start | bytes 3076

commit v2 on v1

--- a/solution.py
+++ b/solution.py
@@ -42,19 +42,16 @@
     matrix_in,
     normal_in,
     stab_in,
-    stream_out,
-    matrix_out,
-    normal_out,
-    stab_out,
+    result,
+    matrix,
+    normal,
+    stab,
     x_own,
     w_in,
     w_gate,
     bias,
     w_out,
     gain,
-    matrix,
-    normal,
-    stab,
     x_all,
     qk_part,
     qk_recv,
@@ -73,9 +70,7 @@
     y_own,
     queries_ref,
     keys_ref,
-    result,
     load_sem,
-    store_sem,
     send_sem,
     recv_sem,
 ):
@@ -100,12 +95,12 @@
         loads.append(copy)
         return copy
 
-    rows = w_gate.shape[1]
+    rows = w_gate.shape[2]
     got_x = load(stream, x_own)
     got_w, got_gate, got_out, got_matrix = [], [], [], []
     for b in range(blocks):
         got_w.append([load(w.at[b], w_in.at[b, n]) for n, w in enumerate((wq, wk, wv, wo))])
-        got_gate.append(load(gate_weight.at[b, pl.ds(pl.multiple_of(di * rows, rows), rows)], w_gate.at[b]))
+        got_gate.append(load(gate_weight.at[b, :, pl.ds(pl.multiple_of(di * rows, rows), rows)], w_gate.at[b]))
         if b == 0:
             got_small = [load(gate_bias, bias), load(norm_gain, gain), load(normal_in, normal), load(stab_in, stab)]
         got_matrix.append(load(matrix_in.at[b], matrix.at[b]))
@@ -113,16 +108,17 @@
 
     barrier = pltpu.get_barrier_semaphore()
 
-    def greet(k):
-        other = lax.rem(ti * dp + di + 1 + k, tp * dp)
-        pl.semaphore_signal(
-            barrier,
-            inc=1,
-            device_id={"tp": other // dp, "dp": lax.rem(other, dp)},
-            device_id_type=pl.DeviceIdType.MESH,
-        )
-
-    each(tp * dp - 1, greet)
+    def greet(where):
+        pl.semaphore_signal(barrier, inc=1, device_id=where, device_id_type=pl.DeviceIdType.MESH)
+
+    def to_others(tell):
+        def along(t, first):
+            each(dp - first, lambda d: tell({"tp": t, "dp": lax.rem(di + first + d, dp)}))
+
+        each(tp - 1, lambda k: along(lax.rem(ti + 1 + k, tp), 0))
+        along(ti, 1)
+
+    to_others(greet)
     pl.semaphore_wait(barrier, tp * dp - 1)
 
     unsent = []
@@ -184,11 +180,16 @@
         return held.reshape(dp * seqs, held.shape[-1])
 
     def moments(stats):
-        means, squares = stats[..., 0:1], stats[..., 1:2]
-        mean = jnp.sum(means, axis=-3) * (1.0 / tp)
-        apart = means - jnp.expand_dims(mean, -3)
-        variance = (jnp.sum(squares, axis=-3) + feats * jnp.sum(apart * apart, axis=-3)) * (1.0 / model)
-        return mean, lax.rsqrt(variance + norm_eps)
+        def column(row, at):
+            shape = (seqs, row.shape[-1])
+            pick = lax.broadcasted_iota(jnp.int32, shape, 1) == lax.broadcasted_iota(jnp.int32, shape, 0) + at
+            return jnp.sum(jnp.where(pick, jnp.broadcast_to(row, shape), 0.0), axis=-1, keepdims=True)
+
+        sums = jnp.sum(stats, axis=0)
+        apart = stats - sums[None] * (1.0 / tp)
+        spread = jnp.sum(apart * apart, axis=0)
+        variance = (column(sums, seqs) + feats * column(spread, 0)) * (1.0 / model)
+        return column(sums, 0) * (1.0 / tp), lax.rsqrt(variance + norm_eps)
 
     def gain_of(b, chunk):
         if len(gain.shape) == 2:
@@ -198,12 +199,6 @@
     got_x.wait()
     to_group(x_own, x_all, 0, STREAM)
     own = x_own[...].astype(f32)
-    outs = []
-
-    def store(src, dst):
-        copy = pltpu.make_async_copy(src, dst, store_sem.at[len(outs)])
-        copy.start()
-        outs.append(copy)
 
     for b in range(blocks):
         if b == 0:
@@ -213,8 +208,8 @@
         chunks = [rows_of(x_all, b, c) for c in range(ratio)]
         if b > 0:
             await_bytes(stat_all.at[b - 1, pl.ds(0, tp * dp - 1)], recv_sem.at[b - 1, STAT])
-            mean, scale = moments(stat_all[b - 1].reshape(dp, tp, seqs, 128))
-            mean, scale = mean.reshape(dp * seqs, 1), scale.reshape(dp * seqs, 1)
+            pairs = [moments(stat_all[b - 1, i * tp : (i + 1) * tp]) for i in range(dp)]
+            mean, scale = (jnp.concatenate(columns, axis=0) for columns in zip(*pairs))
             chunks = [
                 (chunk - mean) * scale * gain_of(b - 1, di * ratio + c) for c, chunk in enumerate(chunks)
             ]
@@ -230,17 +225,20 @@
             for copy in got_w[b][:2]:
                 copy.wait()
         for n in range(2):
-            qk_part[b, :, n] = project(w_in.at[b, n]).reshape(dp, seqs, cols)
+            qk_part[b, :, n] = project(w_in.at[b, n]).reshape(dp, seqs, cols).astype(bf16)
         qk_recv[b, di] = qk_part[b, di]
         to_dp(qk_part, qk_recv, b, QK)
         got_gate[b].wait()
-        g_part[b] = project(w_gate.at[b]).reshape(dp, seqs, 2 * heads)
+        pre = lax.dot_general(
+            jnp.concatenate(chunks, axis=-1), w_gate[b], (((1,), (1,)), ((), ())), preferred_element_type=f32
+        )
+        g_part[b] = pre.reshape(dp, seqs, 2 * heads)
         g_recv[b, di] = g_part[b, di]
         to_dp(g_part, g_recv, b, GATE)
         for copy in got_w[b][2:]:
             copy.wait()
         for n in range(2):
-            vo_part[b, :, n] = project(w_in.at[b, 2 + n]).reshape(dp, seqs, cols)
+            vo_part[b, :, n] = project(w_in.at[b, 2 + n]).reshape(dp, seqs, cols).astype(bf16)
         vo_recv[b, di] = vo_part[b, di]
         to_dp(vo_part, vo_recv, b, VO)
         if b > 0:
@@ -249,7 +247,7 @@
 
         await_bytes(qk_recv.at[b, pl.ds(0, dp - 1)], recv_sem.at[b, QK])
         for n in range(2):
-            total = jnp.sum(qk_recv[b, :, n], axis=0)
+            total = jnp.sum(qk_recv[b, :, n].astype(f32), axis=0)
             for p in range(pieces):
                 head_own[b, n, p] = total[:, p * width : (p + 1) * width].astype(bf16)
         head_all[b, ti] = head_own[b]
@@ -269,8 +267,8 @@
         retain = jnp.exp(carried - stab_new).T
         admit = jnp.exp(log_in - stab_new).T
         await_bytes(vo_recv.at[b, pl.ds(0, dp - 1)], recv_sem.at[b, VO])
-        value = jnp.sum(vo_recv[b, :, 0], axis=0).astype(bf16).astype(f32).T
-        outgate = jnp.sum(vo_recv[b, :, 1], axis=0).astype(bf16).astype(f32)
+        value = jnp.sum(vo_recv[b, :, 0].astype(f32), axis=0).astype(bf16).astype(f32).T
+        outgate = jnp.sum(vo_recv[b, :, 1].astype(f32), axis=0).astype(bf16).astype(f32)
         opened = jax.nn.sigmoid(outgate)
         got_matrix[b].wait()
 
@@ -301,49 +299,37 @@
             readout = jnp.where(lane == s, read.reshape(chans * heads, 1), readout)
         hid_own[b] = (readout.T * opened).astype(bf16)
         to_group(hid_own.at[b], hid_all, b, HID)
-        store(matrix.at[b], matrix_out.at[b])
 
         got_out[b].wait()
         from_group(hid_all, b, HID)
         chunks = [rows_of(hid_all, b, c).astype(bf16) for c in range(ratio)]
-        out_part[b] = project(w_out.at[b], cols).reshape(dp, seqs, feats)
+        out_part[b] = project(w_out.at[b], cols).reshape(dp, seqs, feats).astype(bf16)
         out_recv[b, di] = out_part[b, di]
         to_dp(out_part, out_recv, b, OUT)
         await_bytes(out_recv.at[b, pl.ds(0, dp - 1)], recv_sem.at[b, OUT])
-        y = (residual_scale * own + jnp.sum(out_recv[b], axis=0)).astype(bf16)
+        y = (residual_scale * own + jnp.sum(out_recv[b].astype(f32), axis=0)).astype(bf16)
         y_own[b] = y
         if b + 1 < blocks:
             to_group(y_own.at[b], x_all, b + 1, STREAM)
         y = y.astype(f32)
         mean = jnp.mean(y, axis=-1, keepdims=True)
         square = jnp.sum(jnp.square(y - mean), axis=-1, keepdims=True)
-        at = lax.broadcasted_iota(jnp.int32, (seqs, 128), 1)
-        stat = jnp.where(at == 0, mean, square)
+        lanes = lax.broadcasted_iota(jnp.int32, (seqs, 128), 1)
+        seq = lax.broadcasted_iota(jnp.int32, (seqs, 128), 0)
+        stat = jnp.where(lanes == seq, mean, jnp.where(lanes == seq + seqs, square, 0.0))
+        stat = jnp.sum(stat, axis=0, keepdims=True)
         stat_own[b] = stat
         stat_all[b, di * tp + ti] = stat
 
         if b + 1 < blocks:
 
-            def tell(k, b=b):
-                other = lax.rem(ti * dp + di + 1 + k, tp * dp)
-                send(
-                    stat_own.at[b],
-                    stat_all.at[b, di * tp + ti],
-                    b,
-                    STAT,
-                    {"tp": other // dp, "dp": lax.rem(other, dp)},
-                )
-
-            each(tp * dp - 1, tell)
+            to_others(lambda where: send(stat_own.at[b], stat_all.at[b, di * tp + ti], b, STAT, where))
             unsent.append((tp * dp - 1, stat_own.at[b], b, STAT, None))
         else:
             to_tp(stat_own.at[b], stat_all.at[b, di * tp + ti], b, STAT)
-            store(normal, normal_out)
-            store(stab, stab_out)
             await_bytes(stat_all.at[b, pl.ds(0, tp - 1)], recv_sem.at[b, STAT])
             mean, scale = moments(stat_all[b, pl.ds(di * tp, tp)])
             result[...] = ((y - mean) * scale * gain_of(b, ti)).astype(bf16)
-            store(result, stream_out)
 
     for count, src, b, phase, also in unsent:
         each(count, lambda k: await_bytes(src, send_sem.at[b, phase]))
@@ -353,7 +339,13 @@
             def _():
                 await_bytes(src, send_sem.at[b, phase])
 
-    for copy in outs:
+
+def write_out(*refs):
+    sem = refs[-1]
+    copies = [pltpu.make_async_copy(refs[n], refs[4 + n], sem.at[n]) for n in (1, 2, 0, 3)]
+    for copy in copies:
+        copy.start()
+    for copy in copies:
         copy.wait()
 
 
@@ -382,69 +374,76 @@
     if feats % 128:
         norm_gain = norm_gain.reshape(blocks, tp, feats)
     vmem = pltpu.VMEM
-    anywhere = pl.BlockSpec(memory_space=pl.ANY)
+    far = pl.BlockSpec(memory_space=pltpu.HBM)
+    held = pl.BlockSpec(memory_space=vmem)
     scratch = [
         vmem((seqs, feats), bf16),
         vmem((blocks, 4, rows, cols), bf16),
-        vmem((blocks, rows, 2 * heads), bf16),
+        vmem((blocks, 2 * heads, rows), bf16),
         vmem(gate_bias.shape, f32),
         vmem(output_weight.shape, bf16),
         vmem(norm_gain.shape, f32),
-        vmem(matrix_state.shape, f32),
-        vmem(normalizer_state.shape, f32),
-        vmem(stabilizer_state.shape, f32),
         vmem((blocks, ratio * dp, seqs, feats), bf16),
-        vmem((blocks, dp, 2, seqs, cols), f32),
-        vmem((blocks, dp, 2, seqs, cols), f32),
+        vmem((blocks, dp, 2, seqs, cols), bf16),
+        vmem((blocks, dp, 2, seqs, cols), bf16),
         vmem((blocks, dp, seqs, 2 * heads), f32),
         vmem((blocks, dp, seqs, 2 * heads), f32),
-        vmem((blocks, dp, 2, seqs, cols), f32),
-        vmem((blocks, dp, 2, seqs, cols), f32),
+        vmem((blocks, dp, 2, seqs, cols), bf16),
+        vmem((blocks, dp, 2, seqs, cols), bf16),
         vmem((blocks, 2, pieces, seqs, width), bf16),
         vmem((blocks, tp, 2, pieces, seqs, width), bf16),
         vmem((blocks, seqs, cols), bf16),
         vmem((blocks, ratio * dp, seqs, cols), bf16),
-        vmem((blocks, dp, seqs, feats), f32),
-        vmem((blocks, dp, seqs, feats), f32),
-        vmem((blocks, seqs, 128), f32),
-        vmem((blocks, dp * tp, seqs, 128), f32),
+        vmem((blocks, dp, seqs, feats), bf16),
+        vmem((blocks, dp, seqs, feats), bf16),
+        vmem((blocks, 1, 128), f32),
+        vmem((blocks, dp * tp, 1, 128), f32),
         vmem((blocks, seqs, feats), bf16),
         vmem((seqs, heads, size), f32),
         vmem((seqs, heads, size), f32),
-        vmem((seqs, feats), bf16),
         pltpu.SemaphoreType.DMA((5 + 7 * blocks,)),
-        pltpu.SemaphoreType.DMA((3 + blocks,)),
         pltpu.SemaphoreType.DMA((blocks, 8)),
         pltpu.SemaphoreType.DMA((blocks, 8)),
     ]
-    return pl.pallas_call(
+    results = pl.pallas_call(
         functools.partial(kernel, tp, dp),
         out_shape=(
-            jax.ShapeDtypeStruct(stream.shape, stream.dtype),
-            jax.ShapeDtypeStruct(matrix_state.shape, f32),
-            jax.ShapeDtypeStruct(normalizer_state.shape, f32),
-            jax.ShapeDtypeStruct(stabilizer_state.shape, f32),
+            vmem(stream.shape, bf16),
+            vmem(matrix_state.shape, f32),
+            vmem(normalizer_state.shape, f32),
+            vmem(stabilizer_state.shape, f32),
         ),
-        in_specs=[anywhere] * 12,
-        out_specs=(anywhere,) * 4,
+        in_specs=[far] * 12,
+        out_specs=(held,) * 4,
         scratch_shapes=scratch,
         compiler_params=pltpu.CompilerParams(
-            collective_id=0, has_side_effects=True, vmem_limit_bytes=60 * 1024 * 1024
+            collective_id=0, has_side_effects=True, vmem_limit_bytes=40 * 1024 * 1024
         ),
-    )(
+    )(*(
+        pltpu.with_memory_space_constraint(operand, pltpu.HBM)
+        for operand in (
         stream,
         query_weight,
         key_weight,
         value_weight,
         outgate_weight,
-        gate_weight,
+        jnp.swapaxes(gate_weight, 1, 2),
         gate_bias,
         output_weight,
         norm_gain,
         matrix_state,
         normalizer_state,
         stabilizer_state,
-    )
+        )
+    ))
+    return pl.pallas_call(
+        write_out,
+        out_shape=tuple(jax.ShapeDtypeStruct(r.shape, r.dtype) for r in results),
+        in_specs=[held] * 4,
+        out_specs=(far,) * 4,
+        scratch_shapes=[pltpu.SemaphoreType.DMA((4,))],
+        compiler_params=pltpu.CompilerParams(vmem_limit_bytes=1024 * 1024),
+    )(*results)
 
 
 def solution(mesh):

time: 70.7 us -> 58.5 us (0.83)
  local copies, waits for them, and re-layouts: 11.7 us -> 0 us
    unnamed x9 -> x0, local copies, waits for them, and re-layouts: 11.7 us -> none
    pallas_call x1 -> x2, Pallas kernels: 58.1 us -> 57.7 us  [the longest x1 54.9 us: shards(): pl.pallas_call(functools.partial(kernel, tp, dp), out_shape=(vmem(stream....]
where the time goes in v2:
time: 58.5 us; the launch traced here: 58.4 us
  Pallas kernels  57.7 us (99%)
  between operations  0.64 us (1%)
    pallas_call x1, Pallas kernels, shards(): pl.pallas_call(functools.partial(kernel, tp, dp), out_shape=(vmem(stream....  54.9 us
    pallas_call x1, Pallas kernels, shards(): pl.pallas_call(write_out, out_shape=tuple((jax.ShapeDtypeStruct(r.shape,...  2.81 us

profile of v2, /device:TPU:0, one launch (start us, length us, event | category | flops | bytes accessed | tf_op | source)
XLA Modules:
  0.0 58.4 jit_solution(1010925447194121984)
XLA Ops:
  0.6 54.9 %shard_map.147 = (bf16[8,512]{1,0:T(8,128)(2,1)S(1)}, f32[2,8,24,16,192]{4,3,2,1,0:T(8,128)S(1)}, f32[2,8,16,192]{3,2,1,0:T(8,128)S(1)}, f32[2,8,16]{2,1,0:T(8,128)S(1)}) custom-call(bf16[8,512]{1,0:T(8,128)(2,1)} %stream.1, bf16[2,1024,384]{2,1,0:T(8,128)(2,1)} %wq.1, bf16[2,1024,384]{2,1,0:T(8,128)(2,1)} %wk.1, bf16[2,1024,384]{2,1,0:T(8,128)(2,1)} %wv.1, ...), custom_call_target="tpu_custom_call" | custom-call | tf_op jit(solution)/shard_map/pallas_call | solution.py:408
  55.5 2.8 %shard_map.148 = (bf16[8,512]{1,0:T(8,128)(2,1)}, f32[2,8,24,16,192]{4,3,2,1,0:T(8,128)}, f32[2,8,16,192]{3,2,1,0:T(8,128)}, f32[2,8,16]{2,1,0:T(8,128)}) custom-call(bf16[8,512]{1,0:T(8,128)(2,1)S(1)} %get-tuple-element.8.refs_0_, f32[2,8,24,16,192]{4,3,2,1,0:T(8,128)S(1)} %get-tuple-element.9.refs_1_, f32[2,8,16,192]{3,2,1,0:T(8,128)S(1)} %get-tuple-element.10.refs_2_, ...), custom_call_target="tpu_custom_call" | custom-call | tf_op jit(solution)/shard_map/pallas_call | solution.py:439
